TPU v7x, 32 devices: a whole 2x2x4 slice. The times are simulated.
32 devices in a mesh: dp: 4 (over y, x), kv: 4 (over z), tp: 2 (over core).
Axes of the slice: x: 2, y: 2, z: 4, core: 2. Of those that a mesh axis runs over, the one named last changes fastest.
Arguments:
- tokens: bfloat16 [24, 4096], P('dp', 'kv'), may hold values from -64 to 64
- lengths: int32 [24], P('dp'), may hold values from 128 to 1024, as said below
- attn_gain: float32 [4096], P('kv'), may hold values from 0.1 to 1.9
- query_weight: bfloat16 [4096, 4096], P('kv', 'tp'), may hold values from -0.09375 to 0.09375
- key_weight: bfloat16 [4096, 256], P('kv', 'tp'), may hold values from -0.1875 to 0.1875
- value_weight: bfloat16 [4096, 256], P('kv', 'tp'), may hold values from -0.09375 to 0.09375
- forget_weight: bfloat16 [4096, 4], replicated, may hold values from -0.25 to 0.25
- forget_offset: float32 [4], P('tp'), may hold values from -6 to 0
- cache_keys: bfloat16 [24, 1024, 256], P('dp', 'kv', 'tp'), may hold values from -1600 to 1600
- cache_values: bfloat16 [24, 1024, 256], P('dp', 'kv', 'tp'), may hold values from -6 to 6
- gate_sum: float32 [24, 4, 1024], P('dp', 'tp', 'kv'), may hold values from -82 to 0
- out_weight: bfloat16 [4096, 4096], P('tp', 'kv'), may hold values from -0.1875 to 0.1875
- mlp_gain: float32 [4096], replicated, may hold values from 0.1 to 1.9
- up_weight: bfloat16 [4096, 16384], P(None, ('kv', 'tp')), may hold values from -0.09375 to 0.09375
- down_weight: bfloat16 [16384, 4096], P(('kv', 'tp')), may hold values from -0.0625 to 0.0625
Outputs:
- mixed: bfloat16 [24, 4096], P('dp', ('kv', 'tp'))
Inputs may be any that keep to these rules, and one draw needn't show every extreme that they name: `lengths`: in every draw some sequence has all 1024 positions cached.
All inputs are finite; a program needn't handle non-finite values.
Results may differ from a plain program's by a relative error of at most 0.023.
Values may be sent and summed in bfloat16 or wider, within the bound.
A program may use at most 128 MiB of HBM per device.

v0:
```python
import jax
import jax.numpy as jnp
from jax import lax
from jax.sharding import PartitionSpec as P

D = 4096
HEADS = 64
HD = 64
KEY_VALUE_HEADS = 4
epsilon = 1e-06
floor_score = -1e30


def combined_all(x, axis, combine):
    everything = jax.tree.map(
        lambda part, kind: lax.all_gather(part.astype(kind), axis),
        x,
        (jnp.bfloat16, jnp.bfloat16, jnp.bfloat16),
    )

    def take(k):
        return jax.tree.map(lambda part, own: part[k].astype(own.dtype), everything, x)

    return lax.fori_loop(
        1, lax.axis_size(axis), lambda k, so_far: combine(so_far, take(k)), take(0)
    )


def combine_parts(earlier, later):
    first_top, first_total, first_values = earlier
    second_top, second_total, second_values = later
    merged_top = jnp.maximum(first_top, second_top)
    first_scale = jnp.exp(first_top - merged_top)
    second_scale = jnp.exp(second_top - merged_top)
    first_wide = jnp.repeat(first_scale, HD, axis=1)
    second_wide = jnp.repeat(second_scale, HD, axis=1)
    return (
        merged_top,
        first_total * first_scale + second_total * second_scale,
        first_values * first_wide + second_values * second_wide,
    )


def shards(
    tokens,
    lengths,
    attn_gain,
    query_weight,
    key_weight,
    value_weight,
    forget_weight,
    forget_offset,
    cache_keys,
    cache_values,
    gate_sum,
    out_weight,
    mlp_gain,
    up_weight,
    down_weight,
):
    row_count = tokens.shape[0]
    feature_cols = tokens.shape[1]
    kv_place = lax.axis_index("kv")
    tp_place = lax.axis_index("tp")
    local_heads = key_weight.shape[1] // HD
    group_size = HEADS // KEY_VALUE_HEADS
    token_rows = tokens.astype(jnp.float32)
    scaled_rows = (token_rows * attn_gain[None, :]).astype(jnp.bfloat16)
    square_part = jnp.sum(token_rows * token_rows, axis=1)
    query_part = jnp.dot(scaled_rows, query_weight, preferred_element_type=jnp.float32)
    key_part = jnp.dot(scaled_rows, key_weight, preferred_element_type=jnp.float32)
    value_part = jnp.dot(scaled_rows, value_weight, preferred_element_type=jnp.float32)
    gate_rows = lax.dynamic_slice(
        forget_weight,
        (kv_place * feature_cols, tp_place * local_heads),
        (feature_cols, local_heads),
    )
    forget_part = jnp.dot(scaled_rows, gate_rows, preferred_element_type=jnp.float32)
    query_sum, key_sum, value_sum, forget_sum, square_sum = lax.psum(
        (query_part, key_part, value_part, forget_part, square_part), "kv"
    )
    row_scale = lax.rsqrt(square_sum / D + epsilon)[:, None]
    queries = (query_sum * row_scale).astype(jnp.bfloat16)
    new_key = (key_sum * row_scale).astype(jnp.bfloat16)
    new_value = (value_sum * row_scale).astype(jnp.bfloat16)
    log_forget = jax.nn.log_sigmoid(forget_sum * row_scale + forget_offset[None, :])
    positions_here = cache_keys.shape[1]
    key_heads = cache_keys.reshape(row_count, positions_here, local_heads, HD)
    value_heads = cache_values.reshape(row_count, positions_here, local_heads, HD)
    query_heads = queries.reshape(row_count, local_heads, group_size, HD)
    scores = jnp.einsum(
        "skgd,spkd->skgp", query_heads, key_heads, preferred_element_type=jnp.float32
    ) * HD ** (-0.5)
    scores = scores + gate_sum[:, :, None, :] + log_forget[:, :, None, None]
    cache_pos = kv_place * positions_here + jnp.arange(positions_here)
    active_mask = (cache_pos[None, :] < lengths[:, None])[:, None, None, :]
    local_top = jnp.max(jnp.where(active_mask, scores, floor_score), axis=3)
    weights = jnp.where(active_mask, jnp.exp(scores - local_top[..., None]), 0.0)
    local_total = jnp.sum(weights, axis=3)
    local_values = jnp.einsum(
        "skgp,spkd->skgd",
        weights.astype(jnp.bfloat16),
        value_heads,
        preferred_element_type=jnp.float32,
    )
    head_cols = local_heads * group_size
    merged_top, merged_total, merged_values = combined_all(
        (
            local_top.reshape(row_count, head_cols),
            local_total.reshape(row_count, head_cols),
            local_values.reshape(row_count, head_cols * HD),
        ),
        "kv",
        combine_parts,
    )
    own_score = jnp.einsum(
        "skgd,skd->skg",
        query_heads,
        new_key.reshape(row_count, local_heads, HD),
        preferred_element_type=jnp.float32,
    ).reshape(row_count, head_cols) * HD ** (-0.5)
    final_top = jnp.maximum(merged_top, own_score)
    past_scale = jnp.exp(merged_top - final_top)
    own_weight = jnp.exp(own_score - final_top)
    totals = merged_total * past_scale + own_weight
    own_rounded = lax.optimization_barrier(own_weight.astype(jnp.bfloat16)).astype(jnp.float32)
    own_values = jnp.broadcast_to(
        new_value.astype(jnp.float32).reshape(row_count, local_heads, 1, HD),
        (row_count, local_heads, group_size, HD),
    ).reshape(row_count, head_cols * HD)
    weighted = (
        merged_values * jnp.repeat(past_scale, HD, axis=1)
        + jnp.repeat(own_rounded, HD, axis=1) * own_values
    )
    attended = (weighted / jnp.repeat(totals, HD, axis=1)).astype(jnp.bfloat16)
    partial_out = jnp.dot(attended, out_weight, preferred_element_type=jnp.float32)
    head_sum = lax.psum(partial_out.astype(jnp.bfloat16), "tp").astype(jnp.float32)
    mid_cols = (token_rows + head_sum).astype(jnp.bfloat16)
    mid_rows = lax.all_gather(mid_cols, "kv", axis=1, tiled=True)
    mid_wide = mid_rows.astype(jnp.float32)
    normed_mid = (
        mid_wide
        * mlp_gain[None, :]
        * lax.rsqrt(jnp.mean(mid_wide * mid_wide, axis=1, keepdims=True) + epsilon)
    ).astype(jnp.bfloat16)
    hidden = jnp.square(
        jax.nn.relu(jnp.dot(normed_mid, up_weight, preferred_element_type=jnp.float32))
    ).astype(jnp.bfloat16)
    mixer_term = jnp.dot(hidden, down_weight, preferred_element_type=jnp.float32)
    kv_count = lax.axis_size("kv")
    tp_count = lax.axis_size("tp")
    block_cols = mixer_term.shape[1] // (kv_count * tp_count)
    reordered = (
        mixer_term.reshape(row_count, kv_count, tp_count, block_cols)
        .transpose(0, 2, 1, 3)
        .reshape(row_count, kv_count * tp_count * block_cols)
    )
    pair_share = lax.psum_scatter(
        reordered.astype(jnp.bfloat16), "tp", scatter_dimension=1, tiled=True
    ).astype(jnp.float32)
    mixer_share = lax.psum_scatter(pair_share, "kv", scatter_dimension=1, tiled=True)
    out_cols = mixer_share.shape[1]
    start_col = (kv_place * tp_count + tp_place) * out_cols
    mid_share = lax.dynamic_slice_in_dim(mid_wide, start_col, out_cols, 1)
    return (mid_share + mixer_share).astype(jnp.bfloat16)


def solution(mesh):
    placed = (
        P("dp", "kv"),
        P("dp"),
        P("kv"),
        P("kv", "tp"),
        P("kv", "tp"),
        P("kv", "tp"),
        P(),
        P("tp"),
        P("dp", "kv", "tp"),
        P("dp", "kv", "tp"),
        P("dp", "tp", "kv"),
        P("tp", "kv"),
        P(),
        P(None, ("kv", "tp")),
        P(("kv", "tp"), None),
    )
    return jax.shard_map(
        shards, mesh=mesh, in_specs=placed, out_specs=P("dp", ("kv", "tp")), check_vma=False
    )
```

profile of v0, /device:TPU:0, one launch (start us, length us, event | category | flops | bytes accessed | tf_op | source)
XLA Modules:
  0.0 151.1 jit_solution(10252514063055072850)
XLA Ops:
  6.6 0.9 fusion.20
  7.4 2.9 %fusion.30 = f32[6,2048]{1,0:T(8,128)S(1)} fusion(bf16[1024,2048]{1,0:T(8,128)(2,1)} %param.20, bf16[6,1024]{1,0:T(8,128)(2,1)} %param.17, f32[1024]{0:T(1024)} %param.19), kind=kOutput, calls=%fused_computation.47 | convolution fusion | flops 25184256 | bytes 4259840 | tf_op jit(solution)/shard_map/dot_general | solution.py:70
  10.3 0.9 fusion.24
  11.2 1.1 fusion.26
  12.3 0.9 fusion.28
  13.3 22.1 %all-reduce = (f32[6,2048]{1,0:T(8,128)S(1)}, f32[6]{0:T(128)S(1)}, f32[6,128]{1,0:T(8,128)S(1)}, f32[6,2]{0,1:T(2,128)S(1)}, f32[6,128]{1,0:T(8,128)S(1)}) all-reduce(f32[6,2048]{1,0:T(8,128)S(1)} %fusion.30, f32[6]{0:T(128)S(1)} %fusion.20, f32[6,128]{1,0:T(8,128)S(1)} %fusion.26, ...), channel_id=1, replica_groups=mesh['dp'=4,'kv'=4,'tp'=2] {'kv'}, use_global_device_ids=true, to_apply=%region_0.0 | all-reduce | flops 13842 | bytes 110736 | tf_op jit(solution)/shard_map/psum | solution.py:79
  35.4 0.1 reshape.143
  35.5 0.7 fusion.39
  36.3 0.1 copy.25
  36.4 1.2 copy.24
  37.5 1.2 copy.26
  38.7 0.7 broadcast_compare_fusion
  39.4 1.0 select_reduce_fusion
  40.4 0.2 fusion.8
  40.6 0.3 convolution_convert_fusion.1
  40.9 0.1 convert_element_type.173
  41.0 13.6 %all_gather.17 = bf16[4,6,2048]{2,1,0:T(8,128)(2,1)S(1)} all-gather(bf16[1,6,2048]{2,1,0:T(8,128)(2,1)S(1)} %convert_element_type.173), channel_id=1, replica_groups=mesh['dp'=4,'kv'=4,'tp'=2] {'kv'}, dimensions={0}, use_global_device_ids=true | all-gather | bytes 122880 | tf_op jit(solution)/shard_map/all_gather | solution.py:16
  54.7 11.9 %all_gather.16 = bf16[4,6,32]{2,1,0:T(8,128)(2,1)S(1)} all-gather(bf16[1,6,32]{2,1,0:T(8,128)(2,1)S(1)} %convert_element_type.168), channel_id=1, replica_groups=mesh['dp'=4,'kv'=4,'tp'=2] {'kv'}, dimensions={0}, use_global_device_ids=true | all-gather | bytes 1920 | tf_op jit(solution)/shard_map/all_gather | solution.py:16
  66.7 11.9 %all_gather.15 = bf16[4,6,32]{2,1,0:T(8,128)(2,1)S(1)} all-gather(bf16[1,6,32]{2,1,0:T(8,128)(2,1)S(1)} %convert_element_type.164), channel_id=1, replica_groups=mesh['dp'=4,'kv'=4,'tp'=2] {'kv'}, dimensions={0}, use_global_device_ids=true | all-gather | bytes 1920 | tf_op jit(solution)/shard_map/all_gather | solution.py:16
  78.6 1.3 while.19
  80.1 0.1 fusion.44
  80.3 0.1 broadcast_in_dim.71
  81.1 2.8 %convolution_convert_fusion.2 = bf16[6,1024]{1,0:T(8,128)(2,1)S(1)} fusion(bf16[2048,1024]{1,0:T(8,128)(2,1)} %param.28, f32[6,2048]{1,0:T(8,128)S(1)} %reshape.150, f32[6,2048]{1,0:T(8,128)S(1)} %reshape.148, f32[6,2048]{1,0:T(8,128)S(1)} %reshape.149, f32[6,2048]{1,0:T(8,128)S(1)} %get-tuple-element.183, f32[6,2048]{1,0:T(8,128)S(1)} %reshape.147), kind=kOutput, calls=%fused_computation.16 | convolution fusion | flops 25233408 | bytes 4452352 | tf_op jit(solution)/shard_map/dot_general | solution.py:136
  83.9 3.4 %psum.47 = bf16[6,1024]{1,0:T(8,128)(2,1)S(1)} all-reduce(bf16[6,1024]{1,0:T(8,128)(2,1)S(1)} %convolution_convert_fusion.2), channel_id=1, replica_groups=mesh['dp'=4,'kv'=4,'tp'=2] {'tp'}, use_global_device_ids=true, to_apply=%region_10.11 | all-reduce | flops 6144 | bytes 24576 | tf_op jit(solution)/shard_map/psum | solution.py:137
  87.3 13.1 %all_gather.18 = bf16[6,4096]{1,0:T(8,128)(2,1)S(1)} all-gather(bf16[6,1024]{1,0:T(8,128)(2,1)S(1)} %fusion.21), channel_id=1, replica_groups=mesh['dp'=4,'kv'=4,'tp'=2] {'kv'}, dimensions={1}, use_global_device_ids=true | all-gather | bytes 61440 | tf_op jit(solution)/shard_map/all_gather | solution.py:139
  100.4 0.1 multiply_reduce_fusion
  100.6 12.9 %convolution_convert_fusion = bf16[6,4096]{1,0:T(8,128)(2,1)S(1)} fusion(bf16[2048,4096]{1,0:T(8,128)(2,1)} %param.31, bf16[4096,2048]{1,0:T(8,128)(2,1)} %param.30, f32[6]{0:T(128)S(1)} %add_rsqrt_fusion, f32[4096]{0:T(1024)S(1)} %copy-done.2, bf16[6,4096]{1,0:T(8,128)(2,1)S(1)} %all_gather.18), kind=kOutput, calls=%fused_computation.8 | convolution fusion | flops 201486336 | bytes 33669144 | tf_op jit(solution)/shard_map/dot_general | solution.py:149
  113.6 0.7 convert_element_type.190
  114.3 5.9 %reduce-scatter.3.cloned.1.call-done = bf16[6,2048]{1,0:T(8,128)(2,1)} async-done(((bf16[6,4096]{1,0:T(8,128)(2,1)}), bf16[6,2048]{1,0:T(8,128)(2,1)}) %reduce-scatter.3.cloned.1.call-update) | async-done | bytes 24592 | tf_op jit(solution)/shard_map/reduce_scatter | solution.py:158
  120.2 1.4 convert_element_type.191
  121.6 21.3 %reduce-scatter.5.cloned.1.call-done = f32[6,512]{1,0:T(8,128)} async-done(((f32[6,2048]{1,0:T(8,128)}), f32[6,512]{1,0:T(8,128)}) %reduce-scatter.5.cloned.1.call-update) | async-done | bytes 12304 | tf_op jit(solution)/shard_map/reduce_scatter | solution.py:161
  142.9 1.3 add_convert_fusion
  (55 shorter events, 2.5 us)
Async XLA Ops:
  6.5 3.8 %copy-start = (bf16[1024,128]{1,0:T(8,128)(2,1)S(1)}, bf16[1024,128]{1,0:T(8,128)(2,1)}, u32[]{:S(2)}) copy-start(bf16[1024,128]{1,0:T(8,128)(2,1)} %param.22) | copy-start | bytes 786436
  6.5 80.7 %copy-start.1 = (bf16[6,1024]{1,0:T(8,128)(2,1)S(1)}, bf16[6,1024]{1,0:T(8,128)(2,1)}, u32[]{:S(2)}) copy-start(bf16[6,1024]{1,0:T(8,128)(2,1)} %param.17) | copy-start | bytes 36868
  6.5 94.1 %copy-start.2 = (f32[4096]{0:T(1024)S(1)}, f32[4096]{0:T(1024)}, u32[]{:S(2)}) copy-start(f32[4096]{0:T(1024)} %param.29) | copy-start | bytes 49156
  6.5 113.7 %reduce-scatter.3.cloned.1.call-start = ((), (), s32[]{:S(2)}) async-start(), calls=%async_computation.2 | async-start | bytes 98304 | tf_op jit(solution)/shard_map/reduce_scatter | solution.py:158
  114.3 28.6 %reduce-scatter.5.cloned.1.call-start = ((), (), s32[]{:S(2)}) async-start(), calls=%async_computation.3 | async-start | bytes 81920 | tf_op jit(solution)/shard_map/reduce_scatter | solution.py:161
Sparse Core Ops, SparseCore 0:
  114.4 5.7 reduce-scatter.2
  122.5 20.4 reduce-scatter.4
where the time goes:
time: 152 us; the launch traced here: 151 us
  blocking collectives  76 us (50%)
  waiting for transfers between devices  27.2 us (18%)
  matrix products  22.9 us (15%)
  between operations  13.6 us (9%)
  other arithmetic  5.77 us (4%)
  local copies, waits for them, and re-layouts  5.52 us (4%)
    all_gather x3, blocking collectives, combined_all(): lax.all_gather(part.astype(kind), axis)  37.4 us
    psum x1, blocking collectives, shards(): lax.psum((query_part, key_part, value_part, forget_part, square_part), 'kv')  22.1 us
    reduce_scatter x1, waiting for transfers between devices, shards(): lax.psum_scatter(pair_share, 'kv', scatter_dimension=1, tiled=True)  21.3 us
    all_gather x1, blocking collectives, shards(): mid_rows = lax.all_gather(mid_cols, 'kv', axis=1, tiled=True)  13.1 us
    dot_general x1, matrix products, shards(): jnp.dot(hidden, down_weight, preferred_element_type=jnp.float32)  12.9 us
    reduce_scatter x1, waiting for transfers between devices, shards(): lax.psum_scatter(reordered.astype(jnp.bfloat16), 'tp', scatter_dimension=...  5.88 us
    psum x1, blocking collectives, shards(): lax.psum(partial_out.astype(jnp.bfloat16), 'tp').astype(jnp.float32)  3.36 us
  transfers between devices with their start and end apart: 2, of which 2 were waited for; matrix products, arithmetic and copies ran while one was open for 0% of the time, Pallas kernels for 0%

commit v1 on v0

--- a/solution.py
+++ b/solution.py
@@ -9,6 +9,37 @@
 KEY_VALUE_HEADS = 4
 epsilon = 1e-06
 floor_score = -1e30
+
+
+def search_the_bench(view, axis_no):
+    next_value = list(view.shape[1:])
+    next_value[axis_no] *= view.shape[0]
+    b_now = jnp.moveaxis(view, 0, axis_no).reshape(next_value)
+    return b_now
+
+
+def _see_levels_all(across, array_axis, payload):
+    n_shards = lax.axis_size(across)
+    copies = []
+    for q in range(n_shards):
+        copies.append((q, (q + 1) % n_shards))
+    store = []
+    for w, no in copies:
+        store.append((no, w))
+    mid_arr, oldest = ([], [])
+    for idx in range(n_shards - 1):
+        if idx % 2 == 0:
+            mid_arr.append(
+                lax.ppermute(mid_arr[-1] if mid_arr else payload, axis_name=across, perm=copies)
+            )
+        else:
+            oldest.append(lax.ppermute(oldest[-1] if oldest else payload, across, store))
+    y = jnp.stack([*mid_arr[::-1], payload, *oldest])
+    block_out = lax.axis_index(across)
+    passed = block_out - len(mid_arr)
+    y = y[(jnp.arange(n_shards) - passed) % n_shards]
+    block_now = search_the_bench(y, array_axis)
+    return block_now
 
 
 def combined_all(x, axis, combine):
@@ -136,7 +167,7 @@
     partial_out = jnp.dot(attended, out_weight, preferred_element_type=jnp.float32)
     head_sum = lax.psum(partial_out.astype(jnp.bfloat16), "tp").astype(jnp.float32)
     mid_cols = (token_rows + head_sum).astype(jnp.bfloat16)
-    mid_rows = lax.all_gather(mid_cols, "kv", axis=1, tiled=True)
+    mid_rows = _see_levels_all("kv", 1, mid_cols)
     mid_wide = mid_rows.astype(jnp.float32)
     normed_mid = (
         mid_wide

time: 152 us -> 150 us (0.987)
  blocking collectives: 76 us -> 62.8 us
  waiting for transfers between devices: 27.2 us -> 34.4 us
  starting transfers between devices: 0.04 us -> 3.92 us
    all_gather x1 -> x0, blocking collectives: 13.1 us -> none  [shards(): mid_rows = lax.all_gather(mid_cols, 'kv', axis=1, tiled=True)]
    ppermute x0 -> x3, waiting for transfers between devices: none -> 7.22 us  [the longest x2 7.21 us: _see_levels_all(): lax.ppermute(mid_arr[-1] if mid_arr else payload, axis_name=across, perm=...]
    ppermute x0 -> x3, starting transfers between devices: none -> 3.87 us  [the longest x1 3.81 us: _see_levels_all(): lax.ppermute(oldest[-1] if oldest else payload, across, store)]
  transfers between devices with their start and end apart: 2 -> 5, of which waited for: 2 -> 4; matrix products, arithmetic and copies ran while one was open for 0% -> 0% of each run, Pallas kernels for 0% -> 0%
where the time goes in v1:
time: 150 us
  blocking collectives  62.8 us (42%)
  waiting for transfers between devices  34.4 us (23%)
  matrix products  22.9 us (15%)
  between operations  13.6 us (9%)
  local copies, waits for them, and re-layouts  6.07 us (4%)
  other arithmetic  5.81 us (4%)
  starting transfers between devices  3.92 us (3%)
    all_gather x3, blocking collectives, combined_all(): lax.all_gather(part.astype(kind), axis)  37.4 us
    psum x1, blocking collectives, shards(): lax.psum((query_part, key_part, value_part, forget_part, square_part), 'kv')  22.1 us
    reduce_scatter x1, waiting for transfers between devices, shards(): lax.psum_scatter(pair_share, 'kv', scatter_dimension=1, tiled=True)  21.3 us
    dot_general x1, matrix products, shards(): jnp.dot(hidden, down_weight, preferred_element_type=jnp.float32)  12.9 us
    ppermute x2, waiting for transfers between devices, _see_levels_all(): lax.ppermute(mid_arr[-1] if mid_arr else payload, axis_name=across, perm=...  7.21 us
    reduce_scatter x1, waiting for transfers between devices, shards(): lax.psum_scatter(reordered.astype(jnp.bfloat16), 'tp', scatter_dimension=...  5.85 us
    ppermute x1, starting transfers between devices, _see_levels_all(): lax.ppermute(oldest[-1] if oldest else payload, across, store)  3.81 us
    psum x1, blocking collectives, shards(): lax.psum(partial_out.astype(jnp.bfloat16), 'tp').astype(jnp.float32)  3.36 us
  transfers between devices with their start and end apart: 5, of which 4 were waited for; matrix products, arithmetic and copies ran while one was open for 0% of the time, Pallas kernels for 0%

profile of v1, /device:TPU:0, one launch (start us, length us, event | category | flops | bytes accessed | tf_op | source)
XLA Modules:
  0.0 149.6 jit_solution(17419905353608560941)
XLA Ops:
  6.6 0.9 fusion.18
  7.4 2.9 %fusion.28 = f32[6,2048]{1,0:T(8,128)S(1)} fusion(bf16[1024,2048]{1,0:T(8,128)(2,1)} %param.20, bf16[6,1024]{1,0:T(8,128)(2,1)} %param.17, f32[1024]{0:T(1024)} %param.19), kind=kOutput, calls=%fused_computation.47 | convolution fusion | flops 25184256 | bytes 4259840 | tf_op jit(solution)/shard_map/dot_general | solution.py:101
  10.3 0.9 fusion.22
  11.2 1.1 fusion.24
  12.3 0.9 fusion.26
  13.3 22.1 %all-reduce = (f32[6,2048]{1,0:T(8,128)S(1)}, f32[6]{0:T(128)S(1)}, f32[6,128]{1,0:T(8,128)S(1)}, f32[6,2]{0,1:T(2,128)S(1)}, f32[6,128]{1,0:T(8,128)S(1)}) all-reduce(f32[6,2048]{1,0:T(8,128)S(1)} %fusion.28, f32[6]{0:T(128)S(1)} %fusion.18, f32[6,128]{1,0:T(8,128)S(1)} %fusion.24, ...), channel_id=1, replica_groups=mesh['dp'=4,'kv'=4,'tp'=2] {'kv'}, use_global_device_ids=true, to_apply=%region_0.0 | all-reduce | flops 13842 | bytes 110736 | tf_op jit(solution)/shard_map/psum | solution.py:110
  35.5 0.7 fusion.37
  36.4 1.2 copy.24
  37.5 1.2 copy.26
  38.7 0.7 broadcast_compare_fusion
  39.4 1.0 select_reduce_fusion
  40.4 0.2 fusion.8
  40.6 0.3 convolution_convert_fusion.1
  40.9 0.1 convert_element_type.183
  41.0 13.6 %all_gather.14 = bf16[4,6,2048]{2,1,0:T(8,128)(2,1)S(1)} all-gather(bf16[1,6,2048]{2,1,0:T(8,128)(2,1)S(1)} %convert_element_type.183), channel_id=1, replica_groups=mesh['dp'=4,'kv'=4,'tp'=2] {'kv'}, dimensions={0}, use_global_device_ids=true | all-gather | bytes 122880 | tf_op jit(solution)/shard_map/all_gather | solution.py:47
  54.7 11.9 %all_gather.13 = bf16[4,6,32]{2,1,0:T(8,128)(2,1)S(1)} all-gather(bf16[1,6,32]{2,1,0:T(8,128)(2,1)S(1)} %convert_element_type.178), channel_id=1, replica_groups=mesh['dp'=4,'kv'=4,'tp'=2] {'kv'}, dimensions={0}, use_global_device_ids=true | all-gather | bytes 1920 | tf_op jit(solution)/shard_map/all_gather | solution.py:47
  66.7 11.9 %all_gather.12 = bf16[4,6,32]{2,1,0:T(8,128)(2,1)S(1)} all-gather(bf16[1,6,32]{2,1,0:T(8,128)(2,1)S(1)} %convert_element_type.174), channel_id=1, replica_groups=mesh['dp'=4,'kv'=4,'tp'=2] {'kv'}, dimensions={0}, use_global_device_ids=true | all-gather | bytes 1920 | tf_op jit(solution)/shard_map/all_gather | solution.py:47
  78.6 1.3 while.19
  80.1 0.1 fusion.44
  81.1 2.8 %convolution_convert_fusion.2 = bf16[6,1024]{1,0:T(8,128)(2,1)S(1)} fusion(bf16[2048,1024]{1,0:T(8,128)(2,1)} %param.28, f32[6,2048]{1,0:T(8,128)S(1)} %reshape.202, f32[6,2048]{1,0:T(8,128)S(1)} %reshape.200, f32[6,2048]{1,0:T(8,128)S(1)} %reshape.201, f32[6,2048]{1,0:T(8,128)S(1)} %get-tuple-element.183, f32[6,2048]{1,0:T(8,128)S(1)} %reshape.199), kind=kOutput, calls=%fused_computation.17 | convolution fusion | flops 25233408 | bytes 4452352 | tf_op jit(solution)/shard_map/dot_general | solution.py:167
  83.9 3.4 %psum.47 = bf16[6,1024]{1,0:T(8,128)(2,1)S(1)} all-reduce(bf16[6,1024]{1,0:T(8,128)(2,1)S(1)} %convolution_convert_fusion.2), channel_id=1, replica_groups=mesh['dp'=4,'kv'=4,'tp'=2] {'tp'}, use_global_device_ids=true, to_apply=%region_10.11 | all-reduce | flops 6144 | bytes 24576 | tf_op jit(solution)/shard_map/psum | solution.py:168
  87.4 3.8 %collective-permute-start.2 = (bf16[6,1024]{1,0:T(8,128)(2,1)S(1)}, bf16[6,1024]{1,0:T(8,128)(2,1)S(1)}, u32[]{:S(2)}, u32[]{:S(2)}) collective-permute-start(bf16[6,1024]{1,0:T(8,128)(2,1)S(1)} %fusion.19), channel_id=1, source_target_pairs={{2,0},{4,2},{6,4},{0,6},{3,1},{5,3},{7,5},{1,7},{10,8},{12,10},{14... | collective-permute-start | bytes 36872 | tf_op jit(solution)/shard_map/ppermute | solution.py:36
  91.2 1.7 %collective-permute-done = bf16[6,1024]{1,0:T(8,128)(2,1)S(1)} collective-permute-done((bf16[6,1024]{1,0:T(8,128)(2,1)S(1)}, bf16[6,1024]{1,0:T(8,128)(2,1)S(1)}, u32[]{:S(2)}, u32[]{:S(2)}) %collective-permute-start) | collective-permute-done | bytes 12320 | tf_op jit(solution)/shard_map/ppermute | solution.py:33
  92.9 5.5 %collective-permute-done.1 = bf16[6,1024]{1,0:T(8,128)(2,1)S(1)} collective-permute-done((bf16[6,1024]{1,0:T(8,128)(2,1)S(1)}, bf16[6,1024]{1,0:T(8,128)(2,1)S(1)}, u32[]{:S(2)}, u32[]{:S(2)}) %collective-permute-start.1) | collective-permute-done | bytes 12320 | tf_op jit(solution)/shard_map/ppermute | solution.py:33
  98.5 0.6 gather_fusion
  99.0 0.1 multiply_reduce_fusion
  99.2 12.9 %convolution_convert_fusion = bf16[6,4096]{1,0:T(8,128)(2,1)S(1)} fusion(bf16[2048,4096]{1,0:T(8,128)(2,1)} %param.31, bf16[4096,2048]{1,0:T(8,128)(2,1)} %param.30, f32[6,4096]{1,0:T(8,128)S(1)} %bitcast.61, f32[6]{0:T(128)S(1)} %add_rsqrt_fusion, f32[4096]{0:T(1024)S(1)} %copy-done.2), kind=kOutput, calls=%fused_computation.9 | convolution fusion | flops 201461760 | bytes 33718296 | tf_op jit(solution)/shard_map/dot_general | solution.py:180
  112.2 0.7 convert_element_type.203
  112.9 5.9 %reduce-scatter.3.cloned.1.call-done = bf16[6,2048]{1,0:T(8,128)(2,1)} async-done(((bf16[6,4096]{1,0:T(8,128)(2,1)}), bf16[6,2048]{1,0:T(8,128)(2,1)}) %reduce-scatter.3.cloned.1.call-update) | async-done | bytes 24592 | tf_op jit(solution)/shard_map/reduce_scatter | solution.py:189
  118.8 1.4 convert_element_type.204
  120.2 21.3 %reduce-scatter.5.cloned.1.call-done = f32[6,512]{1,0:T(8,128)} async-done(((f32[6,2048]{1,0:T(8,128)}), f32[6,512]{1,0:T(8,128)}) %reduce-scatter.5.cloned.1.call-update) | async-done | bytes 12304 | tf_op jit(solution)/shard_map/reduce_scatter | solution.py:192
  141.5 1.3 add_convert_fusion
  (64 shorter events, 2.9 us)
Async XLA Ops:
  6.5 3.8 %copy-start = (bf16[1024,128]{1,0:T(8,128)(2,1)S(1)}, bf16[1024,128]{1,0:T(8,128)(2,1)}, u32[]{:S(2)}) copy-start(bf16[1024,128]{1,0:T(8,128)(2,1)} %param.22) | copy-start | bytes 786436
  6.5 80.7 %copy-start.1 = (bf16[6,1024]{1,0:T(8,128)(2,1)S(1)}, bf16[6,1024]{1,0:T(8,128)(2,1)}, u32[]{:S(2)}) copy-start(bf16[6,1024]{1,0:T(8,128)(2,1)} %param.17) | copy-start | bytes 36868
  6.5 92.7 %copy-start.2 = (f32[4096]{0:T(1024)S(1)}, f32[4096]{0:T(1024)}, u32[]{:S(2)}) copy-start(f32[4096]{0:T(1024)} %param.29) | copy-start | bytes 49156
  6.5 112.2 %reduce-scatter.3.cloned.1.call-start = ((), (), s32[]{:S(2)}) async-start(), calls=%async_computation.2 | async-start | bytes 98304 | tf_op jit(solution)/shard_map/reduce_scatter | solution.py:189
  87.3 5.6 %collective-permute-start = (bf16[6,1024]{1,0:T(8,128)(2,1)S(1)}, bf16[6,1024]{1,0:T(8,128)(2,1)S(1)}, u32[]{:S(2)}, u32[]{:S(2)}) collective-permute-start(bf16[6,1024]{1,0:T(8,128)(2,1)S(1)} %fusion.19), channel_id=1, source_target_pairs={{0,2},{2,4},{4,6},{6,0},{1,3},{3,5},{5,7},{7,1},{8,10},{10,12},{12... | collective-permute-start | bytes 36872 | tf_op jit(solution)/shard_map/ppermute | solution.py:33
  87.4 5.5 %collective-permute-start.2 = (bf16[6,1024]{1,0:T(8,128)(2,1)S(1)}, bf16[6,1024]{1,0:T(8,128)(2,1)S(1)}, u32[]{:S(2)}, u32[]{:S(2)}) collective-permute-start(bf16[6,1024]{1,0:T(8,128)(2,1)S(1)} %fusion.19), channel_id=1, source_target_pairs={{2,0},{4,2},{6,4},{0,6},{3,1},{5,3},{7,5},{1,7},{10,8},{12,10},{14... | collective-permute-start | bytes 36872 | tf_op jit(solution)/shard_map/ppermute | solution.py:36
  92.9 5.5 %collective-permute-start.1 = (bf16[6,1024]{1,0:T(8,128)(2,1)S(1)}, bf16[6,1024]{1,0:T(8,128)(2,1)S(1)}, u32[]{:S(2)}, u32[]{:S(2)}) collective-permute-start(bf16[6,1024]{1,0:T(8,128)(2,1)S(1)} %collective-permute-done), channel_id=1, source_target_pairs={{0,2},{2,4},{4,6},{6,0},{1,3},{3,5},{5,7},{7,1},{8,10},{10,12},{12... | collective-permute-start | bytes 36872 | tf_op jit(solution)/shard_map/ppermute | solution.py:33
  112.9 28.6 %reduce-scatter.5.cloned.1.call-start = ((), (), s32[]{:S(2)}) async-start(), calls=%async_computation.3 | async-start | bytes 81920 | tf_op jit(solution)/shard_map/reduce_scatter | solution.py:192
Sparse Core Ops, SparseCore 0:
  113.0 5.7 reduce-scatter.2
  121.0 20.4 reduce-scatter.4
